TPU v7x, 32 devices: a whole 2x2x4 slice. The times are simulated.
32 devices in a mesh: sp: 4 (over y, x), tp: 8 (over z, core).
Axes of the slice: x: 2, y: 2, z: 4, core: 2. Of those that a mesh axis runs over, the one named last changes fastest.
Arguments:
- prompt: bfloat16 [2, 8, 2, 4, 128, 2048], P(None, 'tp', None, 'sp'), may hold values from -60 to 60
- new_token: bfloat16 [2, 2048], replicated, may hold values from -20 to 20
- query_proj_matrix: bfloat16 [2048, 1024], P(None, 'tp'), may hold values from -1 to 1
- key_weight: bfloat16 [2048, 1024], P(None, 'tp'), may hold values from -1 to 1
- value_weight: bfloat16 [2048, 1024], P(None, 'tp'), may hold values from -0.125 to 0.125
- map_balance: float32 [8], replicated, may hold values from 0.3 to 0.8
- head_gain: float32 [128], replicated, may hold values from 0.1 to 1.9
Outputs:
- key_cache: bfloat16 [4, 8, 512, 1024], P('sp', 'tp')
- value_cache: bfloat16 [4, 8, 512, 1024], P('sp', 'tp')
- read: float32 [2, 1024], replicated
All inputs are finite; a program needn't handle non-finite values.
Results may differ from a plain program's by a relative error of at most 0.004.
The roundings to bfloat16 on the way count: a program that leaves them out, or rounds other values in their place, can miss the bound.
Values may be sent and summed in bfloat16 or wider, within the bound.
A program may use at most 64 MiB of HBM per device.

v0:
```python
import jax
import jax.numpy as jnp
from jax import lax
from jax.sharding import PartitionSpec as P

HEADS = 8
MAP_HEAD_SIZE = 64
VD = 128


norm_eps = 1e-06
far_below = -1e30


def joined(part, axis, combine):
    gathered = jax.tree.map(lambda a: lax.all_gather(a, axis), part)

    def take(source):
        return jax.tree.map(lambda a: lax.dynamic_index_in_dim(a, source, 0, False), gathered)

    return lax.fori_loop(
        1, lax.axis_size(axis), lambda source, state: combine(state, take(source)), take(0)
    )


def fill_cols(source, w_piece):
    product = jnp.dot(source, w_piece, preferred_element_type=jnp.float32).astype(jnp.bfloat16)
    return product


def local_new(new_token, query_proj_matrix, key_weight, value_weight):
    return (
        jnp.dot(new_token, query_proj_matrix, preferred_element_type=jnp.float32).astype(
            jnp.bfloat16
        ),
        jnp.dot(new_token, key_weight, preferred_element_type=jnp.float32).astype(jnp.bfloat16),
        jnp.dot(new_token, value_weight, preferred_element_type=jnp.float32).astype(jnp.bfloat16),
    )


def partial_read(query_matrix_rows, key_rows, value_rows):
    logit_scores = jnp.einsum(
        "bhmd,bjhmd->bhmj", query_matrix_rows, key_rows, preferred_element_type=jnp.float32
    ) * MAP_HEAD_SIZE ** (-0.5)
    peak = jnp.max(logit_scores, axis=-1)
    weights_exp = jnp.exp(logit_scores - peak[..., None])
    totals = jnp.sum(weights_exp, axis=-1)
    weighted = jnp.einsum("bhmj,bjhe->bhme", weights_exp, value_rows.astype(jnp.float32))
    return (peak, totals, weighted)


def combine(first, second):
    peak_a, totals_a, weighted_a = first
    peak_b, totals_b, weighted_b = second
    peak = jnp.maximum(peak_a, peak_b)
    factor_a = jnp.exp(peak_a - peak)
    factor_b = jnp.exp(peak_b - peak)
    return (
        peak,
        totals_a * factor_a + totals_b * factor_b,
        weighted_a * factor_a[..., None] + weighted_b * factor_b[..., None],
    )


def shards(prompt, new_token, query_proj_matrix, key_weight, value_weight, map_balance, head_gain):
    seq_count, _, span_count, _, piece_rows, model_width = prompt.shape
    token_rows = prompt.reshape(seq_count * span_count * piece_rows, model_width)
    tp_count = lax.axis_size("tp")
    key_width = key_weight.shape[1] * tp_count
    value_width = value_weight.shape[1] * tp_count
    key_piece = lax.all_gather(key_weight, "tp", axis=1, tiled=True)
    value_piece = lax.all_gather(value_weight, "tp", axis=1, tiled=True)
    key_rows = fill_cols(token_rows, key_piece)
    value_rows = fill_cols(token_rows, value_piece)
    own_columns = local_new(new_token, query_proj_matrix, key_weight, value_weight)
    queries, new_keys, new_values = (
        lax.all_gather(own_columns[0], "tp", axis=1, tiled=True),
        lax.all_gather(own_columns[1], "tp", axis=1, tiled=True),
        lax.all_gather(own_columns[2], "tp", axis=1, tiled=True),
    )
    slot_count = seq_count * span_count
    cached_keys, cached_values = (
        lax.all_to_all(
            key_rows.reshape(slot_count, piece_rows, key_width),
            "sp",
            split_axis=0,
            concat_axis=1,
            tiled=True,
        ),
        lax.all_to_all(
            value_rows.reshape(slot_count, piece_rows, value_width),
            "sp",
            split_axis=0,
            concat_axis=1,
            tiled=True,
        ),
    )
    block_rows = cached_keys.shape[1]
    key_cache = cached_keys.reshape(1, 1, block_rows, key_width)
    value_cache = cached_values.reshape(1, 1, block_rows, value_width)
    all_queries = queries.reshape(seq_count, HEADS, 2, MAP_HEAD_SIZE)
    own_seq = lax.axis_index("sp") // span_count
    own_query = lax.dynamic_slice_in_dim(all_queries, own_seq, 1, 0)
    peak, totals, weighted = partial_read(
        own_query,
        cached_keys.reshape(1, block_rows, HEADS, 2, MAP_HEAD_SIZE),
        cached_values.reshape(1, block_rows, HEADS, VD),
    )
    chosen = jnp.arange(seq_count) == own_seq
    chosen_rows = chosen[:, None, None]
    spread = (
        jnp.where(chosen_rows, peak, far_below),
        jnp.where(chosen_rows, totals, 0.0),
        jnp.where(chosen_rows[..., None], weighted, 0.0),
    )
    merged = joined(spread, ("sp", "tp"), combine)
    own_keys = new_keys.reshape(seq_count, HEADS, 2, MAP_HEAD_SIZE)
    own_score = jnp.einsum(
        "bhmd,bhmd->bhm", all_queries, own_keys, preferred_element_type=jnp.float32
    ) * MAP_HEAD_SIZE ** (-0.5)
    own_values = new_values.astype(jnp.float32).reshape(seq_count, HEADS, VD)
    own_weighted = jnp.broadcast_to(own_values[:, :, None, :], (seq_count, HEADS, 2, VD))
    own_state = (own_score, jnp.ones_like(own_score), own_weighted)
    _, totals, weighted = combine(merged, own_state)
    heads_out = weighted / totals[..., None]
    blended = heads_out[:, :, 0] - map_balance[None, :, None] * heads_out[:, :, 1]
    normed = (
        blended
        * lax.rsqrt(jnp.mean(blended * blended, axis=-1, keepdims=True) + norm_eps)
        * head_gain
    )
    return (key_cache, value_cache, normed.reshape(seq_count, HEADS * VD))


def solution(mesh):
    in_specs = (
        P(None, "tp", None, "sp", None, None),
        P(),
        P(None, "tp"),
        P(None, "tp"),
        P(None, "tp"),
        P(),
        P(),
    )
    out_specs = (P("sp", "tp", None, None), P("sp", "tp", None, None), P())
    return jax.shard_map(shards, mesh=mesh, in_specs=in_specs, out_specs=out_specs, check_vma=False)
```

profile of v0, /device:TPU:0, one launch (start us, length us, event | category | flops | bytes accessed | tf_op | source)
XLA Modules:
  0.0 288.2 jit_solution(11000277364119802212)
XLA Ops:
  7.3 0.7 all-gather.3.cloned.1.call-update
  8.0 0.7 all-gather.5.cloned.1.call-update
  8.7 1.2 convolution_convert_fusion.4
  10.0 13.5 %all_gather.29 = bf16[2,1024]{1,0:T(2,128)(2,1)S(1)} all-gather(bf16[2,128]{1,0:T(2,128)(2,1)S(1)} %convolution_convert_fusion.4), channel_id=1, replica_groups=mesh['sp'=4,'tp'=8] {'tp'}, dimensions={1}, use_global_device_ids=true | all-gather | bytes 4608 | tf_op jit(solution)/shard_map/all_gather | solution.py:77
  23.5 1.2 convolution_convert_fusion.3
  24.7 9.2 %all_gather.33 = bf16[2,1024]{1,0:T(2,128)(2,1)S(1)} all-gather(bf16[2,128]{1,0:T(2,128)(2,1)S(1)} %convolution_convert_fusion.3), channel_id=1, replica_groups=mesh['sp'=4,'tp'=8] {'tp'}, dimensions={1}, use_global_device_ids=true | all-gather | bytes 4608 | tf_op jit(solution)/shard_map/all_gather | solution.py:78
  34.0 0.2 convolution_convert_fusion.2
  34.2 11.9 %all_gather.34 = bf16[2,1024]{1,0:T(2,128)(2,1)S(1)} all-gather(bf16[2,128]{1,0:T(2,128)(2,1)S(1)} %convolution_convert_fusion.2), channel_id=1, replica_groups=mesh['sp'=4,'tp'=8] {'tp'}, dimensions={1}, use_global_device_ids=true | all-gather | bytes 4608 | tf_op jit(solution)/shard_map/all_gather | solution.py:79
  46.3 14.0 %all-gather.3.cloned.1.call-done = bf16[2048,1024]{1,0:T(8,128)(2,1)} async-done(((bf16[2048,128]{1,0:T(8,128)(2,1)}), bf16[2048,1024]{1,0:T(8,128)(2,1)}) %all-gather.3.cloned.1.call-update) | async-done | bytes 4194320 | tf_op jit(solution)/shard_map/all_gather | solution.py:71
  60.2 4.5 %convolution_convert_fusion.1 = bf16[512,1024]{1,0:T(8,128)(2,1)S(1)} fusion(bf16[512,2048]{1,0:T(8,128)(2,1)S(1)} %bitcast.91, bf16[2048,1024]{1,0:T(8,128)(2,1)} %all-gather.3.cloned.1.call-done), kind=kOutput, calls=%fused_computation.11 | convolution fusion | flops 2148007936 | bytes 7340032 | tf_op jit(solution)/shard_map/dot_general | solution.py:27
  64.7 1.3 copy.43
  66.1 3.7 %all-to-all-start = ((bf16[4,128,1024]{1,2,0:T(8,128)(2,1)}), bf16[4,128,1024]{1,2,0:T(8,128)(2,1)S(1)}, u32[]{:S(2)}, u32[]{:S(2)}) async-start(bf16[4,128,1024]{1,2,0:T(8,128)(2,1)} %copy.43), calls=%async_computation | async-start | bytes 2097152 | tf_op jit(solution)/shard_map/all_to_all | solution.py:83
  69.8 38.0 %all-gather.5.cloned.1.call-done = bf16[2048,1024]{1,0:T(8,128)(2,1)} async-done(((bf16[2048,128]{1,0:T(8,128)(2,1)}), bf16[2048,1024]{1,0:T(8,128)(2,1)}) %all-gather.5.cloned.1.call-update) | async-done | bytes 4194320 | tf_op jit(solution)/shard_map/all_gather | solution.py:72
  107.8 5.5 %convolution_convert_fusion = bf16[512,1024]{1,0:T(8,128)(2,1)} fusion(bf16[512,2048]{1,0:T(8,128)(2,1)S(1)} %bitcast.92, bf16[2048,1024]{1,0:T(8,128)(2,1)} %all-gather.5.cloned.1.call-done), kind=kOutput, calls=%fused_computation.10 | convolution fusion | flops 2148007936 | bytes 7340032 | tf_op jit(solution)/shard_map/dot_general | solution.py:27
  113.3 4.2 %all-to-all-start.1 = ((bf16[4,128,1024]{2,1,0:T(8,128)(2,1)}), bf16[4,128,1024]{2,1,0:T(8,128)(2,1)}, u32[]{:S(2)}, u32[]{:S(2)}) async-start(bf16[4,128,1024]{2,1,0:T(8,128)(2,1)} %bitcast.93), calls=%async_computation.1 | async-start | bytes 2097152 | tf_op jit(solution)/shard_map/all_to_all | solution.py:90
  117.6 1.8 copy.45
  119.4 2.3 reshape.114
  121.6 1.5 fusion.11
  123.3 0.2 fusion.6
  123.6 39.7 %all_gather.31 = f32[32,2,8,2]{2,3,1,0:T(2,128)S(1)} all-gather(f32[1,2,8,2]{2,3,1,0:T(2,128)S(1)} %get-tuple-element.222), channel_id=1, replica_groups=mesh['sp'=4,'tp'=8] {'sp','tp'}, dimensions={0}, use_global_device_ids=true | all-gather | bytes 4224 | tf_op jit(solution)/shard_map/all_gather | solution.py:16
  163.3 36.9 %all_gather.30 = f32[32,2,8,2]{2,3,1,0:T(2,128)S(1)} all-gather(f32[1,2,8,2]{2,3,1,0:T(2,128)S(1)} %get-tuple-element.223), channel_id=1, replica_groups=mesh['sp'=4,'tp'=8] {'sp','tp'}, dimensions={0}, use_global_device_ids=true | all-gather | bytes 4224 | tf_op jit(solution)/shard_map/all_gather | solution.py:16
  200.2 1.5 copy.66
  201.7 0.3 fusion.4
  202.1 40.1 %all_gather.32 = f32[32,2,8,2,128]{4,2,3,1,0:T(8,128)S(1)} all-gather(f32[1,2,8,2,128]{4,2,3,1,0:T(8,128)S(1)} %broadcast_select_fusion), channel_id=1, replica_groups=mesh['sp'=4,'tp'=8] {'sp','tp'}, dimensions={0}, use_global_device_ids=true | all-gather | bytes 540672 | tf_op jit(solution)/shard_map/all_gather | solution.py:16
  242.2 0.8 copy-done.2
  243.0 33.5 %while.19 = (s32[]{:T(128)}, f32[2,8,2]{1,2,0:T(2,128)S(1)}, f32[2,8,2]{1,2,0:T(2,128)S(1)}, f32[2,8,2,128]{3,2,1,0:T(2,128)S(1)}, f32[32,2,8,2]{2,3,1,0:T(2,128...) while((s32[]{:T(128)}, f32[2,8,2]{1,2,0:T(2,128)S(1)}, ...), condition=%wide.region_3.4_spmd, body=%wide.region_2.3_spmd.sunk | while | flops 12485 | bytes 83855 | solution.py:21
  243.2 0.7 constant_dynamic-slice_fusion.2
  244.2 0.7 constant_dynamic-slice_fusion.2
  245.0 0.1 fusion.34
  245.3 0.7 constant_dynamic-slice_fusion.2
  246.0 0.1 fusion.34
  246.4 0.7 constant_dynamic-slice_fusion.2
  247.5 0.7 constant_dynamic-slice_fusion.2
  248.2 0.1 fusion.34
  248.6 0.7 constant_dynamic-slice_fusion.2
  249.7 0.7 constant_dynamic-slice_fusion.2
  250.7 0.7 constant_dynamic-slice_fusion.2
  251.8 0.7 constant_dynamic-slice_fusion.2
  252.9 0.7 constant_dynamic-slice_fusion.2
  254.0 0.7 constant_dynamic-slice_fusion.2
  255.1 0.7 constant_dynamic-slice_fusion.2
  256.1 0.7 constant_dynamic-slice_fusion.2
  257.2 0.7 constant_dynamic-slice_fusion.2
  258.3 0.7 constant_dynamic-slice_fusion.2
  259.4 0.7 constant_dynamic-slice_fusion.2
  260.5 0.7 constant_dynamic-slice_fusion.2
  261.5 0.7 constant_dynamic-slice_fusion.2
  262.6 0.7 constant_dynamic-slice_fusion.2
  263.7 0.7 constant_dynamic-slice_fusion.2
  264.8 0.7 constant_dynamic-slice_fusion.2
  265.9 0.7 constant_dynamic-slice_fusion.2
  266.9 0.7 constant_dynamic-slice_fusion.2
  268.0 0.7 constant_dynamic-slice_fusion.2
  269.1 0.7 constant_dynamic-slice_fusion.2
  270.2 0.7 constant_dynamic-slice_fusion.2
  271.3 0.7 constant_dynamic-slice_fusion.2
  272.4 0.7 constant_dynamic-slice_fusion.2
  273.4 0.7 constant_dynamic-slice_fusion.2
  274.5 0.7 constant_dynamic-slice_fusion.2
  275.6 0.7 constant_dynamic-slice_fusion.2
  276.9 0.2 multiply_reduce_fusion
  277.1 0.6 fusion.9
  277.8 1.3 copy.44
  279.1 2.3 copy.112
  (163 shorter events, 11.6 us)
Async XLA Ops:
  7.2 53.1 %copy-start = (bf16[2,1,2,1,128,2048]{5,4,3,2,1,0:T(8,128)(2,1)S(1)}, bf16[2,1,2,1,128,2048]{5,4,3,2,1,0:T(8,128)(2,1)}, u32[]{:S(2)}) copy-start(bf16[2,1,2,1,128,2048]{5,4,3,2,1,0:T(8,128)(2,1)} %param.9) | copy-start | bytes 6291460
  7.2 26.8 %copy-start.1 = (bf16[2048,128]{1,0:T(8,128)(2,1)S(1)}, bf16[2048,128]{1,0:T(8,128)(2,1)}, u32[]{:S(2)}) copy-start(bf16[2048,128]{1,0:T(8,128)(2,1)} %param.13) | copy-start | bytes 1572868
  7.2 26.8 %copy-start.3 = (bf16[2,2048]{1,0:T(2,128)(2,1)S(1)}, bf16[2,2048]{1,0:T(2,128)(2,1)}, u32[]{:S(2)}) copy-start(bf16[2,2048]{1,0:T(2,128)(2,1)} %param.10) | copy-start | bytes 24580
  7.2 39.0 %copy-start.4 = (f32[8]{0:T(128)S(1)}, f32[8]{0:T(128)}, u32[]{:S(2)}) copy-start(f32[8]{0:T(128)} %param.14) | copy-start | bytes 100
  7.2 39.0 %copy-start.5 = (f32[128]{0:T(128)S(1)}, f32[128]{0:T(128)}, u32[]{:S(2)}) copy-start(f32[128]{0:T(128)} %param.15) | copy-start | bytes 1540
  7.2 53.0 %all-gather.3.cloned.1.call-start = ((), (), s32[]{:S(2)}) async-start(), calls=%async_computation.2 | async-start | bytes 4718592 | tf_op jit(solution)/shard_map/all_gather | solution.py:71
  8.0 99.9 %all-gather.5.cloned.1.call-start = ((), (), s32[]{:S(2)}) async-start(), calls=%async_computation.3 | async-start | bytes 4718592 | tf_op jit(solution)/shard_map/all_gather | solution.py:72
  66.1 47.3 %all-to-all-start = ((bf16[4,128,1024]{1,2,0:T(8,128)(2,1)}), bf16[4,128,1024]{1,2,0:T(8,128)(2,1)S(1)}, u32[]{:S(2)}, u32[]{:S(2)}) async-start(bf16[4,128,1024]{1,2,0:T(8,128)(2,1)} %copy.43), calls=%async_computation | async-start | bytes 2097152 | tf_op jit(solution)/shard_map/all_to_all | solution.py:83
  113.3 86.8 %all-to-all-start.1 = ((bf16[4,128,1024]{2,1,0:T(8,128)(2,1)}), bf16[4,128,1024]{2,1,0:T(8,128)(2,1)}, u32[]{:S(2)}, u32[]{:S(2)}) async-start(bf16[4,128,1024]{2,1,0:T(8,128)(2,1)} %bitcast.93), calls=%async_computation.1 | async-start | bytes 2097152 | tf_op jit(solution)/shard_map/all_to_all | solution.py:90
  242.2 0.8 copy-start.2
Sparse Core Ops, SparseCore 0:
  9.6 50.5 all-gather.2
  61.8 45.9 all-gather.4
where the time goes:
time: 291 us; the launch traced here: 288 us
  blocking collectives  151 us (52%)
  waiting for transfers between devices  53.4 us (18%)
  local copies, waits for them, and re-layouts  39.8 us (14%)
  matrix products  14.4 us (5%)
  between operations  14.2 us (5%)
  starting transfers between devices  7.97 us (3%)
  other arithmetic  6.61 us (2%)
    all_gather x3, blocking collectives, joined(): gathered = jax.tree.map(lambda a: lax.all_gather(a, axis), part)  117 us
    all_gather x1, waiting for transfers between devices, shards(): value_piece = lax.all_gather(value_weight, 'tp', axis=1, tiled=True)  38 us
    dynamic_slice x31, local copies, waits for them, and re-layouts, take(): lax.dynamic_index_in_dim(a, source, 0, False)  22.3 us
    all_gather x1, waiting for transfers between devices, shards(): key_piece = lax.all_gather(key_weight, 'tp', axis=1, tiled=True)  14 us
    all_gather x1, blocking collectives, shards(): lax.all_gather(own_columns[0], 'tp', axis=1, tiled=True)  13.5 us
    all_gather x1, blocking collectives, shards(): lax.all_gather(own_columns[2], 'tp', axis=1, tiled=True)  11.9 us
    dot_general x2, matrix products, fill_cols(): jnp.dot(source, w_piece, preferred_element_type=jnp.float32)  10 us
    all_gather x1, blocking collectives, shards(): lax.all_gather(own_columns[1], 'tp', axis=1, tiled=True)  9.21 us
  transfers between devices with their start and end apart: 4, of which 2 were waited for; matrix products, arithmetic and copies ran while one was open for 7% of the time, Pallas kernels for 0%

commit v1 on v0

--- a/solution.py
+++ b/solution.py
@@ -1,6 +1,10 @@
+import functools
+
 import jax
 import jax.numpy as jnp
 from jax import lax
+from jax.experimental import pallas as pl
+from jax.experimental.pallas import tpu as pltpu
 from jax.sharding import PartitionSpec as P
 
 HEADS = 8
@@ -132,6 +136,335 @@
     return (key_cache, value_cache, normed.reshape(seq_count, HEADS * VD))
 
 
+MESH = pl.DeviceIdType.MESH
+CORES = 2
+
+
+def merged_states(states):
+    half = VD // 2
+    peaks = [a[:, VD : VD + 1] for a in states]
+    totals = [a[:, VD + half : VD + half + 1] for a in states]
+    peak = functools.reduce(jnp.maximum, peaks)
+    factors = [jnp.exp(p - peak) for p in peaks]
+    total = functools.reduce(jnp.add, [t * f for t, f in zip(totals, factors)])
+    weighted = functools.reduce(jnp.add, [a[:, :VD] * f for a, f in zip(states, factors)])
+    return weighted, peak, total
+
+
+def packed_state(weighted, peak, total):
+    lane = lax.broadcasted_iota(jnp.int32, weighted.shape, 1)
+    tail = jnp.where(lane < VD // 2, peak, total)
+    return jnp.concatenate([weighted, tail], axis=1)
+
+
+def step_kernel(
+    dims,
+    prompt, token, wq_hbm, wk_hbm, wv_hbm, balance, gain,
+    kout, vout, read,
+    xbuf, wbuf, wq, qbuf, own, stbuf, finbuf,
+    loc, pr_send, pr_recv, line_send, prim_recv, sib_send, sib_recv, xy_send, sec_recv,
+    pk_send, pk_recv, st_send, st_recv, fin_send, fin_recv,
+):
+    sp_count, tp_count, seq_count = dims
+    depth = wbuf.shape[2]
+    cols = wbuf.shape[3] // CORES
+    chips = tp_count // CORES
+    s = lax.axis_index("sp")
+    t = lax.axis_index("tp")
+    z = t // CORES
+    c = t % CORES
+    sib = z * CORES + (1 - c)
+    xs = s + 1 - 2 * (s % 2)
+    ys = (s + 2) % 4
+    prim = (s + s // 2) % 2
+    sec = 1 - prim
+    lanes = pl.ds(pl.multiple_of(c * cols, cols), cols)
+    half = depth // 2
+
+    loads = [
+        pltpu.make_async_copy(wk_hbm, wbuf.at[0, z, :, lanes], loc.at[0]),
+        pltpu.make_async_copy(wv_hbm, wbuf.at[1, z, :, lanes], loc.at[1]),
+        pltpu.make_async_copy(wq_hbm, wq, loc.at[2]),
+        pltpu.make_async_copy(prompt.at[s], xbuf.at[s], loc.at[3]),
+    ]
+    for a in loads:
+        a.start()
+
+    barrier = pltpu.get_barrier_semaphore()
+    for d in range(1, sp_count):
+        pl.semaphore_signal(barrier, inc=1, device_id=((s + d) % sp_count, t), device_id_type=MESH)
+    for d in range(1, tp_count):
+        pl.semaphore_signal(barrier, inc=1, device_id=(s, (t + d) % tp_count), device_id_type=MESH)
+    pl.semaphore_wait(barrier, sp_count + tp_count - 2)
+
+    def remote(src, dst, send, recv, dev):
+        return pltpu.make_async_remote_copy(
+            src_ref=src, dst_ref=dst, send_sem=send, recv_sem=recv, device_id=dev, device_id_type=MESH
+        )
+
+    def block(m, zz):
+        return wbuf.at[m, zz, :, lanes]
+
+    def part(m, zz, h):
+        return wbuf.at[m, zz, pl.ds(h * half, half), lanes]
+
+    sends = []
+
+    def go(copy):
+        copy.start()
+        sends.append(copy)
+
+    loads[0].wait()
+    loads[1].wait()
+
+    def line(direction, zz):
+        return remote(
+            block(prim, zz), block(prim, zz), line_send.at[(direction + 1) // 2, zz], prim_recv.at[zz],
+            (s, t + direction * CORES),
+        )
+
+    def has_next(direction):
+        return (z > 0) if direction < 0 else (z < chips - 1)
+
+    for direction in (-1, 1):
+        pl.when(has_next(direction))(lambda direction=direction: line(direction, z).start())
+    for d in (1, 2, 3):
+        p = xs if d == 1 else ys if d == 2 else 3 - s
+        go(remote(prompt.at[p], xbuf.at[s], pr_send.at[d], pr_recv.at[s], (p, t)))
+    for m in range(2):
+        go(remote(block(m, z), block(m, z), sib_send.at[m, z, 0], sib_recv.at[m, z, 0], (s, sib)))
+
+    loads[2].wait()
+    rows = token[...]
+    me_q = jnp.dot(rows, wq[...], preferred_element_type=jnp.float32)
+    me_k = jnp.dot(rows, wbuf[0, z, :, lanes], preferred_element_type=jnp.float32)
+    me_v = jnp.dot(rows, wbuf[1, z, :, lanes], preferred_element_type=jnp.float32)
+    for i, value in enumerate((me_q, me_k, me_v)):
+        value = value.astype(jnp.bfloat16).astype(jnp.float32)
+        qbuf[t, i * seq_count : (i + 1) * seq_count, :] = value[:seq_count]
+    for d in range(1, tp_count):
+        go(remote(qbuf.at[t], qbuf.at[t], pk_send.at[d], pk_recv.at[t], (s, (t + d) % tp_count)))
+
+    near = jnp.minimum(z, chips - 1 - z)
+
+    def source(j):
+        paired = j <= 2 * near
+        dist = jnp.where(paired, (j + 1) // 2, j - near)
+        from_left = jnp.where(paired, j % 2 == 1, z > near)
+        return jnp.where(from_left, z - dist, z + dist), from_left
+
+    sources = [source(j) for j in range(1, chips)]
+
+    def forwards(from_left):
+        return (
+            jnp.logical_and(from_left, z < chips - 1),
+            jnp.logical_and(jnp.logical_not(from_left), z > 0),
+        )
+
+    def arrive_primary(j):
+        zz, from_left = sources[j]
+        remote(block(prim, zz), block(prim, zz), line_send.at[0, zz], prim_recv.at[zz], (s, t)).wait_recv()
+        for on, direction in zip(forwards(from_left), (1, -1)):
+            pl.when(on)(lambda direction=direction: line(direction, zz).start())
+        go(remote(part(prim, zz, 0), part(prim, zz, 0), xy_send.at[0, zz], sec_recv.at[0, zz], (xs, t)))
+        go(remote(part(prim, zz, 1), part(prim, zz, 1), xy_send.at[1, zz], sec_recv.at[1, zz], (ys, t)))
+        go(remote(block(prim, zz), block(prim, zz), sib_send.at[0, zz, 0], sib_recv.at[0, zz, 0], (s, sib)))
+
+    def arrive_secondary(j):
+        zz, _ = sources[j]
+        for h in range(2):
+            remote(part(sec, zz, h), part(sec, zz, h), xy_send.at[h, zz], sec_recv.at[h, zz], (s, t)).wait_recv()
+            go(remote(part(sec, zz, h), part(sec, zz, h), sib_send.at[1, zz, h], sib_recv.at[1, zz, h], (s, sib)))
+
+    sib_lanes = pl.ds(pl.multiple_of((1 - c) * cols, cols), cols)
+
+    def wait_sibling(m, slot, zz, h):
+        view = wbuf.at[m, zz, :, sib_lanes] if h is None else wbuf.at[m, zz, pl.ds(h * half, half), sib_lanes]
+        h = 0 if h is None else h
+        remote(view, view, sib_send.at[slot, zz, h], sib_recv.at[slot, zz, h], (s, t)).wait_recv()
+
+    def multiply(m, zz):
+        weights = wbuf.at[m, zz]
+        columns = pl.ds(pl.multiple_of(zz * CORES * cols, CORES * cols), CORES * cols)
+
+        def piece(i, _):
+            product = jnp.dot(
+                xbuf[pl.ds(2 * i, 2)].reshape(-1, depth), weights[...], preferred_element_type=jnp.float32
+            ).astype(jnp.bfloat16)
+            at = pl.ds(pl.multiple_of(i * product.shape[0], product.shape[0]), product.shape[0])
+
+            def put(out):
+                out[at, columns] = product
+
+            if isinstance(m, int):
+                put((kout, vout)[m])
+            else:
+                pl.when(m == 0)(lambda: put(kout))
+                pl.when(m == 1)(lambda: put(vout))
+            return 0
+
+        lax.fori_loop(0, sp_count // 2, piece, 0)
+
+    def multiply_primary(j):
+        zz, _ = sources[j]
+        wait_sibling(prim, 0, zz, None)
+        multiply(prim, zz)
+
+    def multiply_secondary(j):
+        zz, _ = sources[j]
+        for h in range(2):
+            wait_sibling(sec, 1, zz, h)
+        multiply(sec, zz)
+
+    last = chips - 1
+    for j in range(min(2, last)):
+        arrive_primary(j)
+
+    for d in range(1, tp_count):
+        i = (t + d) % tp_count
+        remote(qbuf.at[i], qbuf.at[i], pk_send.at[d], pk_recv.at[i], (s, t)).wait_recv()
+    new = jnp.concatenate([qbuf[i] for i in range(tp_count)], axis=1)
+    row = lax.broadcasted_iota(jnp.int32, (2 * HEADS, new.shape[1]), 0)
+    lane = lax.broadcasted_iota(jnp.int32, (2 * HEADS, new.shape[1]), 1)
+    own_lane = lane // MAP_HEAD_SIZE == (row % HEADS) * 2 + row // HEADS
+    scale = MAP_HEAD_SIZE ** (-0.5)
+    short_row = lax.broadcasted_iota(jnp.int32, (2 * HEADS, VD), 0) % HEADS
+
+    def by_head(wide):
+        return functools.reduce(
+            jnp.add,
+            [jnp.where(short_row == h, wide[:, h * VD : (h + 1) * VD], 0.0) for h in range(HEADS)],
+        )
+
+    own_seq = s // (sp_count // seq_count)
+    query = jnp.zeros((2 * HEADS, new.shape[1]), jnp.float32)
+    for b in range(seq_count):
+        q_b = jnp.broadcast_to(new[b : b + 1], query.shape)
+        k_b = jnp.broadcast_to(new[seq_count + b : seq_count + b + 1], query.shape)
+        v_b = jnp.broadcast_to(new[2 * seq_count + b : 2 * seq_count + b + 1], query.shape)
+        score = jnp.sum(jnp.where(own_lane, q_b * k_b, 0.0), axis=1, keepdims=True) * scale
+        own[b] = packed_state(by_head(v_b), score, jnp.ones_like(score))
+        query = jnp.where(own_seq == b, q_b, query)
+    query = jnp.where(own_lane, query, 0.0).astype(jnp.bfloat16)
+
+    loads[3].wait()
+    for d, p in ((1, xs), (2, ys), (3, 3 - s)):
+        remote(xbuf.at[p], xbuf.at[p], pr_send.at[d], pr_recv.at[p], (s, t)).wait_recv()
+    for m in range(2):
+        wait_sibling(m, m, z, None)
+        multiply(m, z)
+    for j in range(last):
+        if j >= 2:
+            arrive_primary(j)
+        multiply_primary(j)
+        if j >= 1:
+            arrive_secondary(j - 1)
+            multiply_secondary(j - 1)
+    arrive_secondary(last - 1)
+    multiply_secondary(last - 1)
+
+    scores = lax.dot_general(
+        query, kout[...], (((1,), (1,)), ((), ())), preferred_element_type=jnp.float32
+    ) * scale
+    peak = jnp.max(scores, axis=1, keepdims=True)
+    raised = jnp.exp(scores - peak)
+    total = jnp.sum(raised, axis=1, keepdims=True)
+    high = raised.astype(jnp.bfloat16)
+    low = (raised - high.astype(jnp.float32)).astype(jnp.bfloat16)
+    wide = jnp.dot(high, vout[...], preferred_element_type=jnp.float32)
+    wide = wide + jnp.dot(low, vout[...], preferred_element_type=jnp.float32)
+    stbuf[t] = packed_state(by_head(wide), peak, total)
+    for d in range(1, tp_count):
+        go(remote(stbuf.at[t], stbuf.at[t], st_send.at[d], st_recv.at[t], (s, (t + d) % tp_count)))
+    for d in range(1, tp_count):
+        i = (t + d) % tp_count
+        remote(stbuf.at[i], stbuf.at[i], st_send.at[d], st_recv.at[i], (s, t)).wait_recv()
+    finbuf[s] = packed_state(*merged_states([stbuf[i] for i in range(tp_count)]))
+    for d in range(1, sp_count):
+        go(remote(finbuf.at[s], finbuf.at[s], fin_send.at[d], fin_recv.at[s], ((s + d) % sp_count, t)))
+    for d in range(1, sp_count):
+        i = (s + d) % sp_count
+        remote(finbuf.at[i], finbuf.at[i], fin_send.at[d], fin_recv.at[i], (s, t)).wait_recv()
+    spans = sp_count // seq_count
+    for b in range(seq_count):
+        weighted, _, total = merged_states([finbuf[b * spans + i] for i in range(spans)] + [own[b]])
+        heads_out = weighted / total
+        blended = heads_out[:HEADS] - balance[...] * heads_out[HEADS:]
+        normed = (
+            blended * lax.rsqrt(jnp.mean(blended * blended, axis=1, keepdims=True) + norm_eps) * gain[...]
+        )
+        for h in range(HEADS):
+            read[b : b + 1, h * VD : (h + 1) * VD] = normed[h : h + 1]
+
+    for direction in (-1, 1):
+        pl.when(has_next(direction))(lambda direction=direction: line(direction, z).wait_send())
+    for zz, from_left in sources:
+        for on, direction in zip(forwards(from_left), (1, -1)):
+            pl.when(on)(lambda direction=direction, zz=zz: line(direction, zz).wait_send())
+    for copy in sends:
+        copy.wait_send()
+
+
+def fused(prompt, new_token, query_proj_matrix, key_weight, value_weight, map_balance, head_gain):
+    seq_count, _, span_count, _, piece_rows, width = prompt.shape
+    sp_count, tp_count = lax.axis_size("sp"), lax.axis_size("tp")
+    cols = key_weight.shape[1]
+    slots = seq_count * span_count
+    chips = tp_count // CORES
+    key_width = cols * tp_count
+    block_rows = sp_count * piece_rows
+    any_space = pl.BlockSpec(memory_space=pl.ANY)
+    vmem = pl.BlockSpec(memory_space=pltpu.VMEM)
+    dma = pltpu.SemaphoreType.DMA
+    keys, values, read = pl.pallas_call(
+        functools.partial(step_kernel, (sp_count, tp_count, seq_count)),
+        out_shape=[
+            jax.ShapeDtypeStruct((block_rows, key_width), jnp.bfloat16),
+            jax.ShapeDtypeStruct((block_rows, key_width), jnp.bfloat16),
+            jax.ShapeDtypeStruct((seq_count, HEADS * VD), jnp.float32),
+        ],
+        in_specs=[any_space, vmem, any_space, any_space, any_space, vmem, vmem],
+        out_specs=[vmem, vmem, vmem],
+        scratch_shapes=[
+            pltpu.VMEM((sp_count, piece_rows, width), jnp.bfloat16),
+            pltpu.VMEM((2, chips, width, CORES * cols), jnp.bfloat16),
+            pltpu.VMEM((width, cols), jnp.bfloat16),
+            pltpu.VMEM((tp_count, 8, cols), jnp.float32),
+            pltpu.VMEM((seq_count, 2 * HEADS, 2 * VD), jnp.float32),
+            pltpu.VMEM((tp_count, 2 * HEADS, 2 * VD), jnp.float32),
+            pltpu.VMEM((sp_count, 2 * HEADS, 2 * VD), jnp.float32),
+            dma((4,)), dma((4,)), dma((sp_count,)), dma((2, chips)), dma((chips,)),
+            dma((2, chips, 2)), dma((2, chips, 2)), dma((2, chips)), dma((2, chips)),
+            dma((tp_count,)), dma((tp_count,)), dma((tp_count,)), dma((tp_count,)),
+            dma((sp_count,)), dma((sp_count,)),
+        ],
+        compiler_params=pltpu.CompilerParams(
+            collective_id=0, has_side_effects=True, vmem_limit_bytes=48 * 1024 * 1024
+        ),
+    )(
+        prompt.reshape(slots, piece_rows, width),
+        new_token, query_proj_matrix, key_weight, value_weight,
+        jnp.broadcast_to(map_balance[:, None], (HEADS, VD)), head_gain[None, :],
+    )
+    shape = (1, 1, block_rows, key_width)
+    return keys.reshape(shape), values.reshape(shape), read
+
+
+def fits(mesh, key_weight, value_weight, prompt):
+    tp_count, sp_count = mesh.shape["tp"], mesh.shape["sp"]
+    seq_count, _, span_count = prompt.shape[:3]
+    cols = key_weight.shape[1] // tp_count
+    return (
+        sp_count == 4
+        and seq_count * span_count == sp_count
+        and tp_count % CORES == 0
+        and tp_count > CORES
+        and cols % VD == 0
+        and 3 * seq_count <= 8
+        and key_weight.shape == value_weight.shape
+    )
+
+
 def solution(mesh):
     in_specs = (
         P(None, "tp", None, "sp", None, None),
@@ -143,4 +476,14 @@
         P(),
     )
     out_specs = (P("sp", "tp", None, None), P("sp", "tp", None, None), P())
-    return jax.shard_map(shards, mesh=mesh, in_specs=in_specs, out_specs=out_specs, check_vma=False)
+
+    def step(prompt, new_token, query_proj_matrix, key_weight, value_weight, map_balance, head_gain):
+        body = fused if fits(mesh, key_weight, value_weight, prompt) else shards
+        mapped = jax.shard_map(
+            body, mesh=mesh, in_specs=in_specs, out_specs=out_specs, check_vma=False
+        )
+        return mapped(
+            prompt, new_token, query_proj_matrix, key_weight, value_weight, map_balance, head_gain
+        )
+
+    return step

time: 291 us -> 80.7 us (0.28)
  blocking collectives: 151 us -> 0 us
  Pallas kernels: 0 us -> 70.4 us
  waiting for transfers between devices: 53.4 us -> 0 us
  local copies, waits for them, and re-layouts: 39.8 us -> 9.33 us
  matrix products: 14.4 us -> 0 us
  between operations: 14.2 us -> 0.65 us
  starting transfers between devices: 7.97 us -> 0 us
  other arithmetic: 6.61 us -> 0 us
    all_gather x6 -> x0, blocking collectives: 151 us -> none  [the longest x3 117 us: joined(): gathered = jax.tree.map(lambda a: lax.all_gather(a, axis), part)]
    pallas_call x0 -> x1, Pallas kernels: none -> 70.4 us  [fused(): pl.pallas_call(functools.partial(step_kernel, (sp_count, tp_count, seq_co...]
    all_gather x2 -> x0, waiting for transfers between devices: 52 us -> none  [the longest x1 38 us: shards(): value_piece = lax.all_gather(value_weight, 'tp', axis=1, tiled=True)]
    dynamic_slice x31 -> x0, local copies, waits for them, and re-layouts: 22.3 us -> none  [take(): lax.dynamic_index_in_dim(a, source, 0, False)]
    dot_general x7 -> x0, matrix products: 14.4 us -> none  [the longest x2 10 us: fill_cols(): jnp.dot(source, w_piece, preferred_element_type=jnp.float32)]
    all_to_all x2 -> x0, starting transfers between devices: 7.9 us -> none  [the longest x1 4.24 us: shards(): lax.all_to_all(value_rows.reshape(slot_count, piece_rows, value_width), '...]
    exp x64 -> x0, local copies, waits for them, and re-layouts: 5.54 us -> none  [the longest x32 2.78 us: combine(): factor_b = jnp.exp(peak_b - peak)]
    add x63 -> x0, other arithmetic: 5.18 us -> none  [the longest x31 4.32 us: combine(): weighted_a * factor_a[..., None] + weighted_b * factor_b[..., None]]
  transfers between devices with their start and end apart: 4 -> 0, of which waited for: 2 -> 0; matrix products, arithmetic and copies ran while one was open for 7% -> 0% of each run, Pallas kernels for 0% -> 0%
where the time goes in v1:
time: 80.7 us; the launch traced here: 80.3 us
  Pallas kernels  70.4 us (87%)
  local copies, waits for them, and re-layouts  9.33 us (12%)
    pallas_call x1, Pallas kernels, fused(): pl.pallas_call(functools.partial(step_kernel, (sp_count, tp_count, seq_co...  70.4 us
    unnamed x15, local copies, waits for them, and re-layouts  8.6 us

profile of v1, /device:TPU:0, one launch (start us, length us, event | category | flops | bytes accessed | tf_op | source)
XLA Modules:
  0.0 80.3 jit_solution(10979543441066822834)
XLA Ops:
  0.6 0.7 broadcast_in_dim.4.balance
  1.4 0.0 copy-start
  1.4 1.6 %copy-done = bf16[2,1,2,1,128,2048]{5,4,3,2,1,0:T(8,128)(2,1)S(1)} copy-done((bf16[2,1,2,1,128,2048]{5,4,3,2,1,0:T(8,128)(2,1)S(1)}, bf16[2,1,2,1,128,2048]{5,4,3,2,1,0:T(8,128)(2,1)}, u32[]{:S(2)}) %copy-start) | copy-done | bytes 2097176
  2.9 0.0 copy-start.1
  2.9 1.0 %copy-done.1 = bf16[2048,128]{1,0:T(8,128)(2,1)S(1)} copy-done((bf16[2048,128]{1,0:T(8,128)(2,1)S(1)}, bf16[2048,128]{1,0:T(8,128)(2,1)}, u32[]{:S(2)}) %copy-start.1) | copy-done | bytes 524312
  4.0 0.0 copy-start.2
  4.0 1.0 %copy-done.2 = bf16[2048,128]{1,0:T(8,128)(2,1)S(1)} copy-done((bf16[2048,128]{1,0:T(8,128)(2,1)S(1)}, bf16[2048,128]{1,0:T(8,128)(2,1)}, u32[]{:S(2)}) %copy-start.2) | copy-done | bytes 524312
  5.0 0.0 copy-start.3
  5.0 1.0 %copy-done.3 = bf16[2048,128]{1,0:T(8,128)(2,1)S(1)} copy-done((bf16[2048,128]{1,0:T(8,128)(2,1)S(1)}, bf16[2048,128]{1,0:T(8,128)(2,1)}, u32[]{:S(2)}) %copy-start.3) | copy-done | bytes 524312
  6.1 0.0 copy-start.4
  6.1 0.7 copy-done.4
  6.8 0.0 copy-start.5
  6.8 0.7 copy-done.5
  7.4 70.4 %shard_map.94 = (bf16[512,1024]{1,0:T(8,128)(2,1)S(1)}, bf16[512,1024]{1,0:T(8,128)(2,1)S(1)}, f32[2,1024]{1,0:T(2,128)S(1)}) custom-call(bf16[4,128,2048]{2,1,0:T(8,128)(2,1)S(1)} %bitcast.4, bf16[2,2048]{1,0:T(2,128)(2,1)S(1)} %copy-done.4, bf16[2048,128]{1,0:T(8,128)(2,1)S(1)} %copy-done.1, bf16[2048,128]{1,0:T(8,128)(2,1)S(1)} %copy-done.2, ...), custom_call_target="tpu_custom_call" | custom-call | tf_op jit(solution)/shard_map/pallas_call | solution.py:419
  77.8 1.0 %copy.13 = bf16[1,1,512,1024]{3,2,1,0:T(8,128)(2,1)} copy(bf16[1,1,512,1024]{3,2,1,0:T(8,128)(2,1)S(1)} %bitcast.6) | data formatting | bytes 2097152
  78.8 1.0 %copy.14 = bf16[1,1,512,1024]{3,2,1,0:T(8,128)(2,1)} copy(bf16[1,1,512,1024]{3,2,1,0:T(8,128)(2,1)S(1)} %bitcast.5) | data formatting | bytes 2097152
  79.7 0.6 copy.15
Async XLA Ops:
  1.4 1.6 %copy-start = (bf16[2,1,2,1,128,2048]{5,4,3,2,1,0:T(8,128)(2,1)S(1)}, bf16[2,1,2,1,128,2048]{5,4,3,2,1,0:T(8,128)(2,1)}, u32[]{:S(2)}) copy-start(bf16[2,1,2,1,128,2048]{5,4,3,2,1,0:T(8,128)(2,1)} %param.7) | copy-start | bytes 6291460
  2.9 1.0 %copy-start.1 = (bf16[2048,128]{1,0:T(8,128)(2,1)S(1)}, bf16[2048,128]{1,0:T(8,128)(2,1)}, u32[]{:S(2)}) copy-start(bf16[2048,128]{1,0:T(8,128)(2,1)} %wq_hbm.1) | copy-start | bytes 1572868
  4.0 1.0 %copy-start.2 = (bf16[2048,128]{1,0:T(8,128)(2,1)S(1)}, bf16[2048,128]{1,0:T(8,128)(2,1)}, u32[]{:S(2)}) copy-start(bf16[2048,128]{1,0:T(8,128)(2,1)} %wk_hbm.1) | copy-start | bytes 1572868
  5.0 1.0 %copy-start.3 = (bf16[2048,128]{1,0:T(8,128)(2,1)S(1)}, bf16[2048,128]{1,0:T(8,128)(2,1)}, u32[]{:S(2)}) copy-start(bf16[2048,128]{1,0:T(8,128)(2,1)} %wv_hbm.1) | copy-start | bytes 1572868
  6.1 0.7 copy-start.4
  6.8 0.7 copy-start.5

commit v2 on v1

--- a/solution.py
+++ b/solution.py
@@ -138,6 +138,7 @@
 
 MESH = pl.DeviceIdType.MESH
 CORES = 2
+PIECES = 2
 
 
 def merged_states(states):
@@ -179,7 +180,8 @@
     prim = (s + s // 2) % 2
     sec = 1 - prim
     lanes = pl.ds(pl.multiple_of(c * cols, cols), cols)
-    half = depth // 2
+    step = depth // PIECES
+    half = step // 2
 
     loads = [
         pltpu.make_async_copy(wk_hbm, wbuf.at[0, z, :, lanes], loc.at[0]),
@@ -205,8 +207,11 @@
     def block(m, zz):
         return wbuf.at[m, zz, :, lanes]
 
-    def part(m, zz, h):
-        return wbuf.at[m, zz, pl.ds(h * half, half), lanes]
+    def piece_of(m, zz, p):
+        return wbuf.at[m, zz, pl.ds(p * step, step), lanes]
+
+    def part(m, zz, p, h):
+        return wbuf.at[m, zz, pl.ds(p * step + h * half, half), lanes]
 
     sends = []
 
@@ -217,9 +222,10 @@
     loads[0].wait()
     loads[1].wait()
 
-    def line(direction, zz):
+    def line(direction, zz, p):
         return remote(
-            block(prim, zz), block(prim, zz), line_send.at[(direction + 1) // 2, zz], prim_recv.at[zz],
+            piece_of(prim, zz, p), piece_of(prim, zz, p),
+            line_send.at[(direction + 1) // 2, zz, p], prim_recv.at[zz, p],
             (s, t + direction * CORES),
         )
 
@@ -227,7 +233,11 @@
         return (z > 0) if direction < 0 else (z < chips - 1)
 
     for direction in (-1, 1):
-        pl.when(has_next(direction))(lambda direction=direction: line(direction, z).start())
+        @pl.when(has_next(direction))
+        def _(direction=direction):
+            for p in range(PIECES):
+                line(direction, z, p).start()
+
     for d in (1, 2, 3):
         p = xs if d == 1 else ys if d == 2 else 3 - s
         go(remote(prompt.at[p], xbuf.at[s], pr_send.at[d], pr_recv.at[s], (p, t)))
@@ -261,27 +271,34 @@
             jnp.logical_and(jnp.logical_not(from_left), z > 0),
         )
 
-    def arrive_primary(j):
+    def arrive_primary(j, p):
         zz, from_left = sources[j]
-        remote(block(prim, zz), block(prim, zz), line_send.at[0, zz], prim_recv.at[zz], (s, t)).wait_recv()
+        view = piece_of(prim, zz, p)
+        remote(view, view, line_send.at[0, zz, p], prim_recv.at[zz, p], (s, t)).wait_recv()
         for on, direction in zip(forwards(from_left), (1, -1)):
-            pl.when(on)(lambda direction=direction: line(direction, zz).start())
-        go(remote(part(prim, zz, 0), part(prim, zz, 0), xy_send.at[0, zz], sec_recv.at[0, zz], (xs, t)))
-        go(remote(part(prim, zz, 1), part(prim, zz, 1), xy_send.at[1, zz], sec_recv.at[1, zz], (ys, t)))
-        go(remote(block(prim, zz), block(prim, zz), sib_send.at[0, zz, 0], sib_recv.at[0, zz, 0], (s, sib)))
+            pl.when(on)(lambda direction=direction: line(direction, zz, p).start())
+        for h, to in enumerate((xs, ys)):
+            view = part(prim, zz, p, h)
+            go(remote(view, view, xy_send.at[h, zz, p], sec_recv.at[h, zz, p], (to, t)))
+        view = piece_of(prim, zz, p)
+        go(remote(view, view, sib_send.at[0, zz, p], sib_recv.at[0, zz, p], (s, sib)))
 
     def arrive_secondary(j):
         zz, _ = sources[j]
-        for h in range(2):
-            remote(part(sec, zz, h), part(sec, zz, h), xy_send.at[h, zz], sec_recv.at[h, zz], (s, t)).wait_recv()
-            go(remote(part(sec, zz, h), part(sec, zz, h), sib_send.at[1, zz, h], sib_recv.at[1, zz, h], (s, sib)))
+        for p in range(PIECES):
+            for h in range(2):
+                view = part(sec, zz, p, h)
+                remote(view, view, xy_send.at[h, zz, p], sec_recv.at[h, zz, p], (s, t)).wait_recv()
+                i = 2 * p + h
+                go(remote(view, view, sib_send.at[1, zz, i], sib_recv.at[1, zz, i], (s, sib)))
 
     sib_lanes = pl.ds(pl.multiple_of((1 - c) * cols, cols), cols)
 
-    def wait_sibling(m, slot, zz, h):
-        view = wbuf.at[m, zz, :, sib_lanes] if h is None else wbuf.at[m, zz, pl.ds(h * half, half), sib_lanes]
-        h = 0 if h is None else h
-        remote(view, view, sib_send.at[slot, zz, h], sib_recv.at[slot, zz, h], (s, t)).wait_recv()
+    def wait_sibling(m, slot, zz, parts):
+        size = depth // parts
+        for i in range(parts):
+            view = wbuf.at[m, zz, pl.ds(i * size, size), sib_lanes]
+            remote(view, view, sib_send.at[slot, zz, i], sib_recv.at[slot, zz, i], (s, t)).wait_recv()
 
     def multiply(m, zz):
         weights = wbuf.at[m, zz]
@@ -307,18 +324,18 @@
 
     def multiply_primary(j):
         zz, _ = sources[j]
-        wait_sibling(prim, 0, zz, None)
+        wait_sibling(prim, 0, zz, PIECES)
         multiply(prim, zz)
 
     def multiply_secondary(j):
         zz, _ = sources[j]
-        for h in range(2):
-            wait_sibling(sec, 1, zz, h)
+        wait_sibling(sec, 1, zz, 2 * PIECES)
         multiply(sec, zz)
 
     last = chips - 1
     for j in range(min(2, last)):
-        arrive_primary(j)
+        for p in range(PIECES):
+            arrive_primary(j, p)
 
     for d in range(1, tp_count):
         i = (t + d) % tp_count
@@ -351,15 +368,21 @@
     for d, p in ((1, xs), (2, ys), (3, 3 - s)):
         remote(xbuf.at[p], xbuf.at[p], pr_send.at[d], pr_recv.at[p], (s, t)).wait_recv()
     for m in range(2):
-        wait_sibling(m, m, z, None)
+        wait_sibling(m, m, z, 1)
         multiply(m, z)
-    for j in range(last):
-        if j >= 2:
-            arrive_primary(j)
-        multiply_primary(j)
-        if j >= 1:
-            arrive_secondary(j - 1)
-            multiply_secondary(j - 1)
+    multiply_primary(0)
+    for j in range(1, last):
+        arrive_secondary(j - 1)
+        later = range(PIECES) if j + 1 < last else ()
+        for p in later:
+            arrive_primary(j + 1, p)
+            if p == 0:
+                multiply_primary(j)
+        if j + 1 == last and last < 3:
+            multiply_primary(j)
+        multiply_secondary(j - 1)
+    if last > 2:
+        multiply_primary(last - 1)
     arrive_secondary(last - 1)
     multiply_secondary(last - 1)
 
@@ -386,21 +409,29 @@
         i = (s + d) % sp_count
         remote(finbuf.at[i], finbuf.at[i], fin_send.at[d], fin_recv.at[i], (s, t)).wait_recv()
     spans = sp_count // seq_count
+    square = (HEADS, HEADS)
+    diagonal = lax.broadcasted_iota(jnp.int32, square, 0) == lax.broadcasted_iota(jnp.int32, square, 1)
+    second = jnp.sum(jnp.where(diagonal, balance[...], 0.0), axis=1, keepdims=True)
     for b in range(seq_count):
         weighted, _, total = merged_states([finbuf[b * spans + i] for i in range(spans)] + [own[b]])
         heads_out = weighted / total
-        blended = heads_out[:HEADS] - balance[...] * heads_out[HEADS:]
+        blended = heads_out[:HEADS] - second * heads_out[HEADS:]
         normed = (
             blended * lax.rsqrt(jnp.mean(blended * blended, axis=1, keepdims=True) + norm_eps) * gain[...]
         )
         for h in range(HEADS):
             read[b : b + 1, h * VD : (h + 1) * VD] = normed[h : h + 1]
 
-    for direction in (-1, 1):
-        pl.when(has_next(direction))(lambda direction=direction: line(direction, z).wait_send())
-    for zz, from_left in sources:
-        for on, direction in zip(forwards(from_left), (1, -1)):
-            pl.when(on)(lambda direction=direction, zz=zz: line(direction, zz).wait_send())
+    for p in range(PIECES):
+        for direction in (-1, 1):
+            pl.when(has_next(direction))(
+                lambda direction=direction, p=p: line(direction, z, p).wait_send()
+            )
+        for zz, from_left in sources:
+            for on, direction in zip(forwards(from_left), (1, -1)):
+                pl.when(on)(
+                    lambda direction=direction, zz=zz, p=p: line(direction, zz, p).wait_send()
+                )
     for copy in sends:
         copy.wait_send()
 
@@ -413,7 +444,7 @@
     chips = tp_count // CORES
     key_width = cols * tp_count
     block_rows = sp_count * piece_rows
-    any_space = pl.BlockSpec(memory_space=pl.ANY)
+    any_space = pl.BlockSpec(memory_space=pltpu.HBM)
     vmem = pl.BlockSpec(memory_space=pltpu.VMEM)
     dma = pltpu.SemaphoreType.DMA
     keys, values, read = pl.pallas_call(
@@ -433,18 +464,19 @@
             pltpu.VMEM((seq_count, 2 * HEADS, 2 * VD), jnp.float32),
             pltpu.VMEM((tp_count, 2 * HEADS, 2 * VD), jnp.float32),
             pltpu.VMEM((sp_count, 2 * HEADS, 2 * VD), jnp.float32),
-            dma((4,)), dma((4,)), dma((sp_count,)), dma((2, chips)), dma((chips,)),
-            dma((2, chips, 2)), dma((2, chips, 2)), dma((2, chips)), dma((2, chips)),
+            dma((4,)), dma((4,)), dma((sp_count,)), dma((2, chips, PIECES)), dma((chips, PIECES)),
+            dma((2, chips, 2 * PIECES)), dma((2, chips, 2 * PIECES)),
+            dma((2, chips, PIECES)), dma((2, chips, PIECES)),
             dma((tp_count,)), dma((tp_count,)), dma((tp_count,)), dma((tp_count,)),
             dma((sp_count,)), dma((sp_count,)),
         ],
         compiler_params=pltpu.CompilerParams(
-            collective_id=0, has_side_effects=True, vmem_limit_bytes=48 * 1024 * 1024
+            collective_id=0, has_side_effects=True, vmem_limit_bytes=62 * 1024 * 1024
         ),
     )(
         prompt.reshape(slots, piece_rows, width),
         new_token, query_proj_matrix, key_weight, value_weight,
-        jnp.broadcast_to(map_balance[:, None], (HEADS, VD)), head_gain[None, :],
+        map_balance[None, :], head_gain[None, :],
     )
     shape = (1, 1, block_rows, key_width)
     return keys.reshape(shape), values.reshape(shape), read

time: 80.7 us -> 71.4 us (0.88)
  local copies, waits for them, and re-layouts: 9.33 us -> 3.93 us
  Pallas kernels: 70.4 us -> 66.6 us
    unnamed x15 -> x7, local copies, waits for them, and re-layouts: 8.6 us -> 3.93 us
    pallas_call x1, Pallas kernels: 70.4 us -> 66.6 us  [fused(): pl.pallas_call(functools.partial(step_kernel, (sp_count, tp_count, seq_co...]
where the time goes in v2:
time: 71.4 us; the launch traced here: 71.2 us
  Pallas kernels  66.6 us (93%)
  local copies, waits for them, and re-layouts  3.93 us (6%)
    pallas_call x1, Pallas kernels, fused(): pl.pallas_call(functools.partial(step_kernel, (sp_count, tp_count, seq_co...  66.6 us
    unnamed x7, local copies, waits for them, and re-layouts  3.93 us

profile of v2, /device:TPU:0, one launch (start us, length us, event | category | flops | bytes accessed | tf_op | source)
XLA Modules:
  0.0 71.2 jit_solution(3407965392508616470)
XLA Ops:
  0.6 66.6 %shard_map.94 = (bf16[512,1024]{1,0:T(8,128)(2,1)}, bf16[512,1024]{1,0:T(8,128)(2,1)}, f32[2,1024]{1,0:T(2,128)}) custom-call(bf16[4,128,2048]{2,1,0:T(8,128)(2,1)} %bitcast.5, bf16[2,2048]{1,0:T(2,128)(2,1)} %token_.1, bf16[2048,128]{1,0:T(8,128)(2,1)} %wq_hbm.1, bf16[2048,128]{1,0:T(8,128)(2,1)} %wk_hbm.1, bf16[2048,128]{1,0:T(8,128)(2,1)} %wv_hbm.1, ...), custom_call_target="tpu_custom_call" | custom-call | tf_op jit(solution)/shard_map/pallas_call | solution.py:450
  67.3 0.0 copy-start
  67.3 0.0 copy-start.1
  67.3 2.3 %copy.13 = bf16[1,1,512,1024]{3,2,1,0:T(8,128)(2,1)} copy(bf16[1,1,512,1024]{3,2,1,0:T(8,128)(2,1)} %bitcast.7) | data formatting | bytes 2097152
  69.6 0.0 copy-done
  69.6 1.0 %copy.14 = bf16[1,1,512,1024]{3,2,1,0:T(8,128)(2,1)} copy(bf16[1,1,512,1024]{3,2,1,0:T(8,128)(2,1)S(1)} %bitcast.6) | data formatting | bytes 2097152
  70.6 0.0 copy-done.1
  70.6 0.6 copy.15
Async XLA Ops:
  67.3 2.4 %copy-start = (bf16[512,1024]{1,0:T(8,128)(2,1)S(1)}, bf16[512,1024]{1,0:T(8,128)(2,1)}, u32[]{:S(2)}) copy-start(bf16[512,1024]{1,0:T(8,128)(2,1)} %get-tuple-element.7) | copy-start | bytes 3145732
  67.3 3.3 %copy-start.1 = (f32[2,1024]{1,0:T(2,128)S(1)}, f32[2,1024]{1,0:T(2,128)}, u32[]{:S(2)}) copy-start(f32[2,1024]{1,0:T(2,128)} %get-tuple-element.14) | copy-start | bytes 24580

commit v3 on v2

--- a/solution.py
+++ b/solution.py
@@ -271,17 +271,24 @@
             jnp.logical_and(jnp.logical_not(from_left), z > 0),
         )
 
+    def primary_copies(j, p):
+        zz, _ = sources[j]
+        copies = []
+        for h, to in enumerate((xs, ys)):
+            view = part(prim, zz, p, h)
+            copies.append(remote(view, view, xy_send.at[h, zz, p], sec_recv.at[h, zz, p], (to, t)))
+        view = piece_of(prim, zz, p)
+        copies.append(remote(view, view, sib_send.at[0, zz, p], sib_recv.at[0, zz, p], (s, sib)))
+        return copies
+
     def arrive_primary(j, p):
         zz, from_left = sources[j]
         view = piece_of(prim, zz, p)
         remote(view, view, line_send.at[0, zz, p], prim_recv.at[zz, p], (s, t)).wait_recv()
         for on, direction in zip(forwards(from_left), (1, -1)):
             pl.when(on)(lambda direction=direction: line(direction, zz, p).start())
-        for h, to in enumerate((xs, ys)):
-            view = part(prim, zz, p, h)
-            go(remote(view, view, xy_send.at[h, zz, p], sec_recv.at[h, zz, p], (to, t)))
-        view = piece_of(prim, zz, p)
-        go(remote(view, view, sib_send.at[0, zz, p], sib_recv.at[0, zz, p], (s, sib)))
+        for copy in primary_copies(j, p):
+            copy.start()
 
     def arrive_secondary(j):
         zz, _ = sources[j]
@@ -336,6 +343,13 @@
     for j in range(min(2, last)):
         for p in range(PIECES):
             arrive_primary(j, p)
+    inside = near > 0
+
+    @pl.when(inside)
+    def _():
+        for j in range(2, last):
+            for p in range(PIECES):
+                arrive_primary(j, p)
 
     for d in range(1, tp_count):
         i = (t + d) % tp_count
@@ -375,7 +389,7 @@
         arrive_secondary(j - 1)
         later = range(PIECES) if j + 1 < last else ()
         for p in later:
-            arrive_primary(j + 1, p)
+            pl.when(jnp.logical_not(inside))(lambda: arrive_primary(j + 1, p))
             if p == 0:
                 multiply_primary(j)
         if j + 1 == last and last < 3:
@@ -432,6 +446,9 @@
                 pl.when(on)(
                     lambda direction=direction, zz=zz, p=p: line(direction, zz, p).wait_send()
                 )
+    for j in range(last):
+        for p in range(PIECES):
+            sends.extend(primary_copies(j, p))
     for copy in sends:
         copy.wait_send()
 
@@ -450,9 +467,9 @@
     keys, values, read = pl.pallas_call(
         functools.partial(step_kernel, (sp_count, tp_count, seq_count)),
         out_shape=[
-            jax.ShapeDtypeStruct((block_rows, key_width), jnp.bfloat16),
-            jax.ShapeDtypeStruct((block_rows, key_width), jnp.bfloat16),
-            jax.ShapeDtypeStruct((seq_count, HEADS * VD), jnp.float32),
+            pltpu.VMEM((block_rows, key_width), jnp.bfloat16),
+            pltpu.VMEM((block_rows, key_width), jnp.bfloat16),
+            pltpu.VMEM((seq_count, HEADS * VD), jnp.float32),
         ],
         in_specs=[any_space, vmem, any_space, any_space, any_space, vmem, vmem],
         out_specs=[vmem, vmem, vmem],
@@ -471,7 +488,7 @@
             dma((sp_count,)), dma((sp_count,)),
         ],
         compiler_params=pltpu.CompilerParams(
-            collective_id=0, has_side_effects=True, vmem_limit_bytes=62 * 1024 * 1024
+            collective_id=0, has_side_effects=True, vmem_limit_bytes=61 * 1024 * 1024 + 800 * 1024
         ),
     )(
         prompt.reshape(slots, piece_rows, width),

time: 71.4 us -> 62.9 us (0.88)
  Pallas kernels: 66.6 us -> 59.6 us
  local copies, waits for them, and re-layouts: 3.93 us -> 2.54 us
    pallas_call x1, Pallas kernels: 66.6 us -> 59.6 us  [fused(): pl.pallas_call(functools.partial(step_kernel, (sp_count, tp_count, seq_co...]
    unnamed x7 -> x3, local copies, waits for them, and re-layouts: 3.93 us -> 2.54 us
where the time goes in v3:
time: 62.9 us; the launch traced here: 62.8 us
  Pallas kernels  59.6 us (95%)
  local copies, waits for them, and re-layouts  2.54 us (4%)
  between operations  0.64 us (1%)
    pallas_call x1, Pallas kernels, fused(): pl.pallas_call(functools.partial(step_kernel, (sp_count, tp_count, seq_co...  59.6 us
    unnamed x3, local copies, waits for them, and re-layouts  2.54 us

profile of v3, /device:TPU:0, one launch (start us, length us, event | category | flops | bytes accessed | tf_op | source)
XLA Modules:
  0.0 62.8 jit_solution(2811238797249538354)
XLA Ops:
  0.6 59.6 %shard_map.94 = (bf16[512,1024]{1,0:T(8,128)(2,1)S(1)}, bf16[512,1024]{1,0:T(8,128)(2,1)S(1)}, f32[2,1024]{1,0:T(2,128)S(1)}) custom-call(bf16[4,128,2048]{2,1,0:T(8,128)(2,1)} %bitcast.7, bf16[2,2048]{1,0:T(2,128)(2,1)} %token_.1, bf16[2048,128]{1,0:T(8,128)(2,1)} %wq_hbm.1, bf16[2048,128]{1,0:T(8,128)(2,1)} %wk_hbm.1, bf16[2048,128]{1,0:T(8,128)(2,1)} %wv_hbm.1, ...), custom_call_target="tpu_custom_call" | custom-call | tf_op jit(solution)/shard_map/pallas_call | solution.py:467
  60.2 1.0 %copy.13 = bf16[1,1,512,1024]{3,2,1,0:T(8,128)(2,1)} copy(bf16[1,1,512,1024]{3,2,1,0:T(8,128)(2,1)S(1)} %bitcast.6) | data formatting | bytes 2097152
  61.2 1.0 %copy.14 = bf16[1,1,512,1024]{3,2,1,0:T(8,128)(2,1)} copy(bf16[1,1,512,1024]{3,2,1,0:T(8,128)(2,1)S(1)} %bitcast.5) | data formatting | bytes 2097152
  62.2 0.6 copy.15
